TPU v7x, 32 devices: a whole 2x2x4 slice. The times are simulated.
32 devices in a mesh: gr: 2 (over x), sp: 8 (over z, y), tp: 2 (over core).
Axes of the slice: x: 2, y: 2, z: 4, core: 2. Of those that a mesh axis runs over, the one named last changes fastest.
Arguments:
- tokens: bfloat16 [16, 512, 4096], P('gr', 'sp'), may hold values from -6 to 6
- key_weight: bfloat16 [4096, 2048], P(('gr', 'sp'), 'tp'), may hold values from -0.09375 to 0.09375
- value_weight: bfloat16 [4096, 2048], P(('gr', 'sp'), 'tp'), may hold values from -0.09375 to 0.09375
- gate_weight: bfloat16 [4096, 16], P(('gr', 'sp'), 'tp'), may hold values from -0.09375 to 0.09375
- forget_bias: float32 [16], P('tp'), may hold values from 7 to 9
- new_query: bfloat16 [16, 16, 128], P('gr', 'tp'), may hold values from -6 to 6
Outputs:
- key_cache: bfloat16 [16, 16, 512, 128], P(('gr', 'sp'), 'tp')
- value_cache: bfloat16 [16, 16, 512, 128], P(('gr', 'sp'), 'tp')
- gate_cache: float32 [16, 16, 512], P(('gr', 'sp'), 'tp')
- first_read: bfloat16 [16, 16, 128], P(('gr', 'sp'), 'tp')
All inputs are finite; a program needn't handle non-finite values.
Results may differ from a plain program's by a relative error of at most 0.0075.
Values may be sent and summed in bfloat16 or wider, within the bound.
A program may use at most 64 MiB of HBM per device.

v0:
```python
import jax
import jax.numpy as jnp
from jax import lax
from jax.sharding import PartitionSpec as P

eps = 1e-06


def taken_in(piece, axis, dim, turn, start):
    def gathered(part):
        return lax.all_gather(part, axis, axis=dim, tiled=True)

    return turn(start, jax.tree.map(gathered, piece), jnp.int32(0))


def carried_in(array, axis, combine, identity, reverse):
    length, mine = lax.axis_size(axis), lax.axis_index(axis)
    everything = jax.tree.map(lambda part: lax.all_gather(part, axis), array)
    start = jax.tree.map(
        lambda part, zero: jnp.broadcast_to(jnp.asarray(zero, part.dtype), part.shape),
        array,
        identity,
    )

    def turn(k, before):
        at = length - 1 - k if reverse else k
        reached = at > mine if reverse else at < mine
        new = combine(before, jax.tree.map(lambda part: part[at], everything))
        return jax.tree.map(lambda a, b: jnp.where(reached, a, b), new, before)

    return lax.fori_loop(0, length, turn, start)


def add_pair(earlier, later):
    return earlier + later


def partial_read(queries, keys, values, cumulative, scaling):
    scores = (
        jnp.einsum("shd,shpd->shp", queries, keys, preferred_element_type=jnp.float32) * scaling
        - cumulative
    )
    highest = jnp.max(scores, axis=2)
    weights = jnp.exp(scores - highest[..., None])
    weight_sum = jnp.sum(weights, axis=2)
    value_sum = jnp.einsum("shp,shpd->shd", weights, values.astype(jnp.float32))
    return (highest, weight_sum, value_sum)


def on_device(tokens, key_weight, value_weight, gate_weight, forget_bias, new_query):
    sequences, positions, features = tokens.shape
    heads_here = forget_bias.shape[0]
    head_dim = new_query.shape[2]
    scaling = head_dim ** (-0.5)
    row_count = sequences * positions
    flat = tokens.reshape(row_count, features)
    empty_kv = jnp.zeros((row_count, key_weight.shape[1]), jnp.float32)
    empty_gate = jnp.zeros((row_count, heads_here), jnp.float32)
    initial = (empty_kv, empty_kv, empty_gate)

    def add_rows(sums, pieces, start):
        columns = lax.dynamic_slice_in_dim(flat, start, pieces[0].shape[0], 1)
        return tuple(
            (
                running + jnp.dot(columns, piece, preferred_element_type=jnp.float32)
                for running, piece in zip(sums, pieces)
            )
        )

    projected = taken_in(
        (key_weight, value_weight, gate_weight), ("gr", "sp"), 0, add_rows, initial
    )
    key_sum, value_sum, gate_logit = projected
    keys = (
        key_sum.astype(jnp.bfloat16)
        .reshape(sequences, positions, heads_here, head_dim)
        .transpose(0, 2, 1, 3)
    )
    values = (
        value_sum.astype(jnp.bfloat16)
        .reshape(sequences, positions, heads_here, head_dim)
        .transpose(0, 2, 1, 3)
    )
    log_gate = jax.nn.log_sigmoid(gate_logit + forget_bias).reshape(
        sequences, positions, heads_here
    )
    running_gate = jnp.cumsum(log_gate.transpose(0, 2, 1), axis=2)
    earlier_sum = carried_in(
        running_gate[:, :, -1],
        "sp",
        add_pair,
        jnp.zeros((sequences, heads_here), jnp.float32),
        False,
    )
    cumulative = running_gate + earlier_sum[:, :, None]
    key_cache, value_cache = (
        lax.all_to_all(keys, "sp", split_axis=0, concat_axis=2, tiled=True),
        lax.all_to_all(values, "sp", split_axis=0, concat_axis=2, tiled=True),
    )
    gate_cache = lax.all_to_all(cumulative, "sp", split_axis=0, concat_axis=2, tiled=True)
    member = lax.axis_index("sp")
    own_query = lax.dynamic_slice_in_dim(new_query, member, 1, 0)
    highest, weight_sum, value_total = partial_read(
        own_query, key_cache, value_cache, gate_cache, scaling
    )
    attended = value_total / weight_sum[..., None]
    normed = attended * lax.rsqrt(jnp.mean(attended * attended, axis=-1, keepdims=True) + eps)
    return (key_cache, value_cache, gate_cache, normed.astype(jnp.bfloat16))


def solution(mesh):
    in_specs = (
        P("gr", "sp", None),
        P(("gr", "sp"), "tp"),
        P(("gr", "sp"), "tp"),
        P(("gr", "sp"), "tp"),
        P("tp"),
        P("gr", "tp", None),
    )
    out_specs = (
        P(("gr", "sp"), "tp", None, None),
        P(("gr", "sp"), "tp", None, None),
        P(("gr", "sp"), "tp", None),
        P(("gr", "sp"), "tp", None),
    )
    return jax.shard_map(
        on_device, mesh=mesh, in_specs=in_specs, out_specs=out_specs, check_vma=False
    )
```

profile of v0, /device:TPU:0, one launch (start us, length us, event | category | flops | bytes accessed | tf_op | source)
XLA Modules:
  0.0 303.1 jit_solution(3733088857924785863)
XLA Ops:
  7.2 0.0 copy-start
  7.2 0.0 all-gather.4.cloned.1.call-start
  7.2 0.7 all-gather.4.cloned.1.call-update
  7.9 0.0 all-gather.6.cloned.1.call-start
  8.0 0.7 all-gather.6.cloned.1.call-update
  8.7 43.3 %all_gather.14 = bf16[4096,8]{0,1:T(8,128)(2,1)S(1)} all-gather(bf16[256,8]{0,1:T(8,128)(2,1)} %param.11), channel_id=1, replica_groups=mesh['gr'=2,'sp'=8,'tp'=2] {'gr','sp'}, dimensions={0}, use_global_device_ids=true | all-gather | bytes 69632 | tf_op jit(solution)/shard_map/all_gather | solution.py:11
  52.0 3.4 %fusion.7 = f32[512,8]{0,1:T(8,128)S(1)} fusion(bf16[512,4096]{1,0:T(8,128)(2,1)} %bitcast.73, bf16[4096,8]{0,1:T(8,128)(2,1)S(1)} %all_gather.14, f32[8]{0:T(128)} %param.12), kind=kOutput, calls=%fused_computation.15 | convolution fusion | flops 33591296 | bytes 4276256 | tf_op jit(solution)/shard_map/dot_general | solution.py:65
  55.4 0.1 reshape.72
  55.5 1.8 reduce_window_sum.11
  57.3 0.1 slice.4
  57.3 0.1 copy.23
  57.5 30.6 %all-gather = f32[64,8,1]{1,2,0:T(1,128)S(1)} all-gather(f32[8,8,1]{1,2,0:T(1,128)S(1)} %copy.23), channel_id=2, replica_groups=mesh['gr'=2,'sp'=8,'tp'=2] {'sp'}, dimensions={0}, use_global_device_ids=true | all-gather | bytes 2304 | tf_op jit(solution)/shard_map/all_gather | solution.py:18
  88.1 0.2 while.14
  88.3 0.1 broadcast_add_fusion
  88.4 0.7 reshape.81
  89.1 3.3 %all-to-all-start.2 = ((f32[8,1,512]{2,1,0:T(1,128)}), f32[8,1,512]{2,1,0:T(1,128)S(1)}, u32[]{:S(2)}, u32[]{:S(2)}) async-start(f32[8,1,512]{2,1,0:T(1,128)} %reshape.81), calls=%async_computation.2 | async-start | bytes 32768 | tf_op jit(solution)/shard_map/all_to_all | solution.py:100
  92.5 34.4 %all-gather.4.cloned.1.call-done = bf16[4096,1024]{1,0:T(8,128)(2,1)} async-done(((bf16[256,1024]{1,0:T(8,128)(2,1)}), bf16[4096,1024]{1,0:T(8,128)(2,1)}) %all-gather.4.cloned.1.call-update) | async-done | bytes 8388624 | tf_op jit(solution)/shard_map/all_gather | solution.py:11
  126.8 9.1 %fusion = bf16[64,8,8,128]{3,1,2,0:T(8,128)(2,1)S(1)} fusion(bf16[512,4096]{1,0:T(8,128)(2,1)} %bitcast.74, bf16[4096,1024]{1,0:T(8,128)(2,1)} %all-gather.4.cloned.1.call-done), kind=kOutput, calls=%fused_computation.3 | convolution fusion | flops 4295491584 | bytes 13631488 | tf_op jit(solution)/shard_map/dot_general | solution.py:65
  136.0 0.3 copy.35
  136.3 1.0 bitcast_bitcast_fusion.1
  137.3 0.0 all-to-all-done.2
  137.3 3.6 %all-to-all-start = ((bf16[8,8,64,128]{3,1,2,0:T(8,128)(2,1)}), bf16[8,8,64,128]{3,1,2,0:T(8,128)(2,1)S(1)}, u32[]{:S(2)}, u32[]{:S(2)}) async-start(bf16[8,8,64,128]{3,1,2,0:T(8,128)(2,1)} %bitcast_bitcast_fusion.1), calls=%async_computation | async-start | bytes 2097152 | tf_op jit(solution)/shard_map/all_to_all | solution.py:97
  140.9 111.6 %all-gather.6.cloned.1.call-done = bf16[4096,1024]{1,0:T(8,128)(2,1)} async-done(((bf16[256,1024]{1,0:T(8,128)(2,1)}), bf16[4096,1024]{1,0:T(8,128)(2,1)}) %all-gather.6.cloned.1.call-update) | async-done | bytes 8388624 | tf_op jit(solution)/shard_map/all_gather | solution.py:11
  252.5 9.1 %fusion.1 = bf16[64,8,8,128]{3,1,2,0:T(8,128)(2,1)S(1)} fusion(bf16[512,4096]{1,0:T(8,128)(2,1)} %bitcast.75, bf16[4096,1024]{1,0:T(8,128)(2,1)} %all-gather.6.cloned.1.call-done), kind=kOutput, calls=%fused_computation.4 | convolution fusion | flops 4295491584 | bytes 13631488 | tf_op jit(solution)/shard_map/dot_general | solution.py:65
  261.7 0.3 copy.36
  262.0 1.0 bitcast_bitcast_fusion
  263.0 0.0 all-to-all-done
  263.0 3.8 %all-to-all-start.1 = ((bf16[8,8,64,128]{3,1,2,0:T(8,128)(2,1)}), bf16[8,8,64,128]{3,1,2,0:T(8,128)(2,1)S(1)}, u32[]{:S(2)}, u32[]{:S(2)}) async-start(bf16[8,8,64,128]{3,1,2,0:T(8,128)(2,1)} %bitcast_bitcast_fusion), calls=%async_computation.1 | async-start | bytes 2097152 | tf_op jit(solution)/shard_map/all_to_all | solution.py:98
  266.8 0.0 copy-done
  266.8 0.5 broadcast.38
  267.3 0.7 reduce.6
  268.0 0.1 reshape.82
  268.1 0.1 all_to_all.53
  268.2 0.7 all_to_all.52
  268.9 0.4 fusion.5
  269.2 0.1 fusion.14
  269.4 0.2 fusion.10
  269.6 0.1 fusion.11
  269.7 23.0 %all-to-all-done.1 = bf16[8,8,64,128]{3,1,2,0:T(8,128)(2,1)S(1)} async-done(((bf16[8,8,64,128]{3,1,2,0:T(8,128)(2,1)}), bf16[8,8,64,128]{3,1,2,0:T(8,128)(2,1)S(1)}, u32[]{:S(2)}, u32[]{:S(2)}) %all-to-all-start.1) | async-done | bytes 1048608 | tf_op jit(solution)/shard_map/all_to_all | solution.py:98
  292.6 0.3 fusion.3
  292.9 0.2 multiply_reduce_fusion
  293.1 0.7 fusion.13
  293.8 1.2 copy.20
  295.0 1.2 copy.21
  (13 shorter events, 0.1 us)
Async XLA Ops:
  7.2 259.6 %copy-start = (bf16[8,8,128]{2,1,0:T(8,128)(2,1)S(1)}, bf16[8,8,128]{2,1,0:T(8,128)(2,1)}, u32[]{:S(2)}) copy-start(bf16[8,8,128]{2,1,0:T(8,128)(2,1)} %param.13) | copy-start | bytes 49156
  7.2 119.7 %all-gather.4.cloned.1.call-start = ((), (), s32[]{:S(2)}) async-start(), calls=%async_computation.3 | async-start | bytes 8912896 | tf_op jit(solution)/shard_map/all_gather | solution.py:11
  7.9 244.6 %all-gather.6.cloned.1.call-start = ((), (), s32[]{:S(2)}) async-start(), calls=%async_computation.4 | async-start | bytes 8912896 | tf_op jit(solution)/shard_map/all_gather | solution.py:11
  89.1 48.2 %all-to-all-start.2 = ((f32[8,1,512]{2,1,0:T(1,128)}), f32[8,1,512]{2,1,0:T(1,128)S(1)}, u32[]{:S(2)}, u32[]{:S(2)}) async-start(f32[8,1,512]{2,1,0:T(1,128)} %reshape.81), calls=%async_computation.2 | async-start | bytes 32768 | tf_op jit(solution)/shard_map/all_to_all | solution.py:100
  137.3 125.7 %all-to-all-start = ((bf16[8,8,64,128]{3,1,2,0:T(8,128)(2,1)}), bf16[8,8,64,128]{3,1,2,0:T(8,128)(2,1)S(1)}, u32[]{:S(2)}, u32[]{:S(2)}) async-start(bf16[8,8,64,128]{3,1,2,0:T(8,128)(2,1)} %bitcast_bitcast_fusion.1), calls=%async_computation | async-start | bytes 2097152 | tf_op jit(solution)/shard_map/all_to_all | solution.py:97
  263.0 29.6 %all-to-all-start.1 = ((bf16[8,8,64,128]{3,1,2,0:T(8,128)(2,1)}), bf16[8,8,64,128]{3,1,2,0:T(8,128)(2,1)S(1)}, u32[]{:S(2)}, u32[]{:S(2)}) async-start(bf16[8,8,64,128]{3,1,2,0:T(8,128)(2,1)} %bitcast_bitcast_fusion), calls=%async_computation.1 | async-start | bytes 2097152 | tf_op jit(solution)/shard_map/all_to_all | solution.py:98
Sparse Core Ops, SparseCore 0:
  10.7 116.0 all-gather.3
  129.6 122.9 all-gather.5
where the time goes:
time: 303 us
  waiting for transfers between devices  170 us (56%)
  blocking collectives  74 us (24%)
  matrix products  22.4 us (7%)
  between operations  14.2 us (5%)
  starting transfers between devices  10.8 us (4%)
  local copies, waits for them, and re-layouts  7.45 us (2%)
  other arithmetic  3.86 us (1%)
    all_gather x2, waiting for transfers between devices, gathered(): return lax.all_gather(part, axis, axis=dim, tiled=True)  146 us
    all_gather x1, blocking collectives, gathered(): return lax.all_gather(part, axis, axis=dim, tiled=True)  43.3 us
    all_gather x1, blocking collectives, carried_in(): everything = jax.tree.map(lambda part: lax.all_gather(part, axis), array)  30.6 us
    all_to_all x1, waiting for transfers between devices, on_device(): lax.all_to_all(values, 'sp', split_axis=0, concat_axis=2, tiled=True)  23 us
    dot_general x3, matrix products, add_rows(): jnp.dot(columns, piece, preferred_element_type=jnp.float32)  21.7 us
  transfers between devices with their start and end apart: 5, of which 3 were waited for; matrix products, arithmetic and copies ran while one was open for 10% of the time, Pallas kernels for 0%

commit v1 on v0

v1 whole, which is shorter than its diff:
```python
import functools

import jax
import jax.numpy as jnp
from jax import lax
from jax.experimental import pallas as pl
from jax.experimental.pallas import tpu as pltpu
from jax.sharding import PartitionSpec as P

eps = 1e-06
MESH = pl.DeviceIdType.MESH


def exchange(
    gr_size, sp_size, tokens, weights, gate_rows, kv_out, gate_out,
    tok, full, gates, staged, gate_staged,
    tok_send, tok_recv, mate_send, mate_recv, w_send, w_recv, z_send, z_recv,
    gw_send, gw_recv, g_send, g_recv, o_send, o_recv, local,
):
    g, s, t = lax.axis_index("gr"), lax.axis_index("sp"), lax.axis_index("tp")
    y, z = lax.rem(s, 2), s // 2
    levels = sp_size // 2
    sequences, positions, features = tokens.shape
    depth, width = weights.shape[1], full.shape[1]
    head_dim = kv_out.shape[2]
    heads = width // head_dim
    members = gr_size * sp_size
    me = g * sp_size + s
    mate = t + 1 - 2 * lax.rem(t, 2)
    core = lax.rem(t, 2)
    quarter = sequences // 4

    gr_of = (g, 1 - g, g, 1 - g)
    y_of = (y, y, 1 - y, 1 - y)

    def where(r, level=None):
        return (gr_of[r], (z if level is None else level) * 2 + y_of[r], t)

    def remote(src, dst, send, recv, device):
        return pltpu.make_async_remote_copy(
            src_ref=src, dst_ref=dst, send_sem=send, recv_sem=recv,
            device_id=device, device_id_type=MESH,
        )

    barrier = pltpu.get_barrier_semaphore()

    def greet(k, carry):
        @pl.when(k != me)
        def _():
            pl.semaphore_signal(
                barrier, inc=1, device_id=(k // sp_size, lax.rem(k, sp_size), t),
                device_id_type=MESH,
            )
        return carry

    lax.fori_loop(0, members, greet, 0)
    pl.semaphore_signal(barrier, inc=1, device_id=(g, s, mate), device_id_type=MESH)
    pl.semaphore_wait(barrier, members)

    def rows_at(r, level):
        return full.at[pl.ds(pl.multiple_of((gr_of[r] * sp_size + level * 2 + y_of[r]) * depth, depth), depth), :]

    def part_for(r):
        return weights.at[gr_of[r], :, pl.ds(pl.multiple_of(y_of[r] * width, width), width)]

    def w_copy(r):
        return remote(part_for(r), rows_at(0, z), w_send.at[r], w_recv.at[r], where(r))

    def w_landing(r):
        return remote(part_for(r), rows_at(r, z), w_send.at[r], w_recv.at[r], where(r))

    def z_copy(direction, r, level, src=None):
        block = rows_at(r, level)
        to = z + 1 if direction == 0 else z - 1
        return remote(
            block if src is None else src, block, z_send.at[direction, level, r],
            z_recv.at[level, r], where(0, to),
        )

    def can_send(direction):
        return z < levels - 1 if direction == 0 else z > 0

    def pass_on(direction, r, level, src=None):
        @pl.when(can_send(direction))
        def _():
            z_copy(direction, r, level, src).start()

    own_part = part_for(0)
    for r in (3, 1, 2):
        w_copy(r).start()
    for direction in range(2):
        pass_on(direction, 0, z, own_part)
    own_rows = pltpu.make_async_copy(own_part, rows_at(0, z), local.at[0])
    own_rows.start()
    own_tokens = pltpu.make_async_copy(tokens, tok.at[0], local.at[1])
    own_tokens.start()

    def gw_copy(k):
        return remote(
            gate_rows, gates.at[me], gw_send.at[k], gw_recv.at[me],
            (k // sp_size, lax.rem(k, sp_size), t),
        )

    def gw_landing(k):
        return remote(
            gate_rows, gates.at[k], gw_send.at[k], gw_recv.at[k],
            (k // sp_size, lax.rem(k, sp_size), t),
        )

    def others(fn):
        def turn(k, carry):
            @pl.when(k != me)
            def _():
                fn(k)
            return carry
        lax.fori_loop(0, members, turn, 0)

    others(lambda k: gw_copy(k).start())
    own_gate = pltpu.make_async_copy(gate_rows, gates.at[me], local.at[2])
    own_gate.start()

    def piece(ref, half, c):
        return ref.at[pl.ds((half * 2 + c) * quarter, quarter)]

    def tok_copy(r, c):
        return remote(
            piece(tokens, core, c), piece(tok.at[r], core, c),
            tok_send.at[r, c], tok_recv.at[r, c], where(r),
        )

    def corner_copy(via, c):
        return remote(
            piece(tok.at[via], core, c), piece(tok.at[3], core, c),
            tok_send.at[3, c], tok_recv.at[3, c], where(3 - via),
        )

    def mate_copy(r, c, half):
        return remote(
            piece(tok.at[r], half, c), piece(tok.at[r], half, c),
            mate_send.at[r, c], mate_recv.at[r, c], (g, s, mate),
        )

    for c in range(2):
        tok_copy(1, c).start()
        tok_copy(2, 1 - c).start()

    def token_arrival(r, c):
        tok_copy(r, c).wait_recv()
        mate_copy(r, c, core).start()

    own_gate.wait()
    own_tokens.wait()
    for r in (1, 2, 3):
        w_landing(r).wait_recv()
        for direction in range(2):
            pass_on(direction, r, z)

    others(lambda k: gw_landing(k).wait_recv())
    gate_full = jnp.concatenate([gates[k] for k in range(members)], axis=1).astype(jnp.bfloat16)

    def gate_copy(k):
        return remote(
            gate_staged.at[k], gate_out.at[s], g_send.at[k], g_recv.at[s], (g, k, t)
        )

    def gate_landing(k):
        return remote(
            gate_staged.at[k], gate_out.at[k], g_send.at[k], g_recv.at[k], (g, k, t)
        )

    def gate_turn(k, carry):
        gate_staged[k] = lax.dot_general(
            gate_full, tok[0, k], (((1,), (1,)), ((), ())),
            preferred_element_type=jnp.float32,
        )
        @pl.when(k != s)
        def _():
            gate_copy(k).start()
        @pl.when(k == s)
        def _():
            pltpu.make_async_copy(gate_staged.at[k], gate_out.at[k], local.at[3]).start()
        return carry

    lax.fori_loop(0, sequences, gate_turn, 0)

    def z_step(j):
        for r in range(4):
            @pl.when(z - j >= 0)
            def _():
                z_copy(0, r, z - j).wait_recv()
                pass_on(0, r, z - j)
            @pl.when(z + j < levels)
            def _():
                z_copy(1, r, z + j).wait_recv()
                pass_on(1, r, z + j)

    z_step(1)
    token_arrival(1, 0)
    corner_copy(1, 0).start()
    token_arrival(2, 1)
    corner_copy(2, 1).start()
    for j in range(2, levels - 1):
        z_step(j)
    token_arrival(1, 1)
    token_arrival(2, 0)
    if levels > 2:
        z_step(levels - 1)
    own_rows.wait()

    tile = min(width, 2 * head_dim)
    tiles = width // tile
    group = min(sequences, max(1, 512 // positions))
    groups = sequences // group

    def out_copy(r, k):
        return remote(
            staged.at[r, :, k],
            kv_out.at[pl.ds((g * 2 + y) * heads, heads), pl.ds(pl.multiple_of((z * 2 + y_of[r]) * positions, positions), positions), :],
            o_send.at[r, k], o_recv.at[me, y_of[r]], (gr_of[r], k, t),
        )

    def out_landing(k, b):
        their_g, their_s = k // sp_size, lax.rem(k, sp_size)
        their_y, their_z = lax.rem(their_s, 2), their_s // 2
        return remote(
            staged.at[0, :, 0],
            kv_out.at[pl.ds((their_g * 2 + their_y) * heads, heads), pl.ds(pl.multiple_of((their_z * 2 + b) * positions, positions), positions), :],
            o_send.at[0, 0], o_recv.at[k, b], (their_g, their_s, t),
        )

    def keep_copy(r):
        return pltpu.make_async_copy(
            staged.at[r, :, s],
            kv_out.at[pl.ds((g * 2 + y) * heads, heads), pl.ds(pl.multiple_of((z * 2 + y_of[r]) * positions, positions), positions), :],
            local.at[4 + r],
        )

    def products(r):
        def turn(i, carry):
            m, n = i // tiles, lax.rem(i, tiles)
            rows = tok[r, pl.ds(m * group, group)].reshape(group * positions, features)
            columns = full[:, pl.ds(pl.multiple_of(n * tile, tile), tile)]
            out = jnp.dot(rows, columns, preferred_element_type=jnp.float32).astype(jnp.bfloat16)
            for h in range(tile // head_dim):
                staged[r, n * (tile // head_dim) + h, pl.ds(m * group, group)] = out[
                    :, h * head_dim : (h + 1) * head_dim
                ].reshape(group, positions, head_dim)
            return carry

        lax.fori_loop(0, groups * tiles, turn, 0)

        def send(i, carry):
            k = lax.rem(s + 1 + i, sp_size)
            if r in (1, 3):
                out_copy(r, k).start()
            else:
                @pl.when(k != s)
                def _():
                    out_copy(r, k).start()
                @pl.when(k == s)
                def _():
                    keep_copy(r).start()
            return carry

        lax.fori_loop(0, sequences, send, 0)

    products(0)
    for r in (1, 2):
        for c in range(2):
            mate_copy(r, c, 1 - core).wait_recv()
        products(r)
    for c in range(2):
        token_arrival(3, c)
    for c in range(2):
        mate_copy(3, c, 1 - core).wait_recv()
    products(3)

    def landed(k):
        for b in range(2):
            out_landing(k, b).wait_recv()

    others(landed)
    keep_copy(0).wait()
    keep_copy(2).wait()

    def gate_landed(k, carry):
        @pl.when(k != s)
        def _():
            gate_landing(k).wait_recv()
            gate_copy(k).wait_send()
        @pl.when(k == s)
        def _():
            pltpu.make_async_copy(gate_staged.at[k], gate_out.at[k], local.at[3]).wait()
        return carry

    lax.fori_loop(0, sequences, gate_landed, 0)
    others(lambda k: gw_copy(k).wait_send())
    for r in (1, 2, 3):
        w_copy(r).wait_send()
        for c in range(2):
            mate_copy(r, c, core).wait_send()
    for c in range(2):
        tok_copy(1, c).wait_send()
        tok_copy(2, c).wait_send()
    corner_copy(1, 0).wait_send()
    corner_copy(2, 1).wait_send()
    for r in range(4):
        def sent(k, carry):
            if r in (1, 3):
                out_copy(r, k).wait_send()
            else:
                @pl.when(k != s)
                def _():
                    out_copy(r, k).wait_send()
            return carry
        lax.fori_loop(0, sequences, sent, 0)
    for r in range(4):
        for direction in range(2):
            @pl.when(can_send(direction))
            def _():
                z_copy(direction, r, z, own_part if r == 0 else None).wait_send()
        for j in range(1, levels):
            @pl.when((z - j >= 0) & can_send(0))
            def _():
                z_copy(0, r, z - j).wait_send()
            @pl.when((z + j < levels) & can_send(1))
            def _():
                z_copy(1, r, z + j).wait_send()


def on_device(gr_size, sp_size, tokens, key_weight, value_weight, gate_weight, forget_bias, new_query):
    sequences, positions, features = tokens.shape
    heads_here = forget_bias.shape[0]
    head_dim = new_query.shape[2]
    scaling = head_dim ** (-0.5)
    members = gr_size * sp_size
    depth = key_weight.shape[0]
    width = 2 * key_weight.shape[1] // 4
    weights = jnp.stack([key_weight, value_weight])
    gate_rows = gate_weight.T.astype(jnp.float32)
    levels = sp_size // 2
    dma = pltpu.SemaphoreType.DMA
    kv, logits = pl.pallas_call(
        functools.partial(exchange, gr_size, sp_size),
        out_shape=(
            jax.ShapeDtypeStruct((2 * heads_here, sp_size * positions, head_dim), jnp.bfloat16),
            jax.ShapeDtypeStruct((sp_size, heads_here, positions), jnp.float32),
        ),
        in_specs=[pl.BlockSpec(memory_space=pl.ANY)] * 3,
        out_specs=(pl.BlockSpec(memory_space=pl.ANY),) * 2,
        scratch_shapes=[
            pltpu.VMEM((4, sequences, positions, features), jnp.bfloat16),
            pltpu.VMEM((features, width), jnp.bfloat16),
            pltpu.VMEM((members, heads_here, depth), jnp.float32),
            pltpu.VMEM((4, width // head_dim, sequences, positions, head_dim), jnp.bfloat16),
            pltpu.VMEM((sequences, heads_here, positions), jnp.float32),
            dma((4, 2)), dma((4, 2)), dma((4, 2)), dma((4, 2)),
            dma((4,)), dma((4,)),
            dma((2, levels, 4)), dma((levels, 4)),
            dma((members,)), dma((members,)),
            dma((sp_size,)), dma((sp_size,)),
            dma((4, sp_size)), dma((members, 2)),
            dma((8,)),
        ],
        compiler_params=pltpu.CompilerParams(
            collective_id=0, has_side_effects=True, vmem_limit_bytes=60 * 1024 * 1024
        ),
    )(tokens, weights, gate_rows)
    key_cache, value_cache = kv[:heads_here], kv[heads_here:]
    logit = logits.transpose(1, 0, 2).reshape(heads_here, sp_size * positions)
    log_gate = jax.nn.log_sigmoid(logit + forget_bias[:, None])
    cumulative = jnp.cumsum(log_gate, axis=1)
    query = lax.dynamic_index_in_dim(new_query, lax.axis_index("sp"), 0, keepdims=False)
    scores = (
        jnp.einsum("hd,hpd->hp", query, key_cache, preferred_element_type=jnp.float32) * scaling
        + cumulative[:, -1:] - cumulative
    )
    highest = jnp.max(scores, axis=1, keepdims=True)
    probs = jnp.exp(scores - highest)
    total = jnp.sum(probs, axis=1)
    attended = jnp.einsum("hp,hpd->hd", probs, value_cache.astype(jnp.float32)) / total[:, None]
    normed = attended * lax.rsqrt(jnp.mean(attended * attended, axis=-1, keepdims=True) + eps)
    return (
        key_cache[None], value_cache[None], cumulative[None], normed.astype(jnp.bfloat16)[None]
    )


def solution(mesh):
    in_specs = (
        P("gr", "sp", None),
        P(("gr", "sp"), "tp"),
        P(("gr", "sp"), "tp"),
        P(("gr", "sp"), "tp"),
        P("tp"),
        P("gr", "tp", None),
    )
    out_specs = (
        P(("gr", "sp"), "tp", None, None),
        P(("gr", "sp"), "tp", None, None),
        P(("gr", "sp"), "tp", None),
        P(("gr", "sp"), "tp", None),
    )
    return jax.shard_map(
        functools.partial(on_device, mesh.shape["gr"], mesh.shape["sp"]),
        mesh=mesh, in_specs=in_specs, out_specs=out_specs, check_vma=False,
    )
```

time: 303 us -> 143 us (0.47)
  waiting for transfers between devices: 170 us -> 0 us
  Pallas kernels: 0 us -> 128 us
  blocking collectives: 74 us -> 0 us
  matrix products: 22.4 us -> 3.21 us
  between operations: 14.2 us -> 0.7 us
  starting transfers between devices: 10.8 us -> 0 us
  local copies, waits for them, and re-layouts: 7.45 us -> 3.44 us
    all_gather x2 -> x0, waiting for transfers between devices: 146 us -> none  [gathered(): return lax.all_gather(part, axis, axis=dim, tiled=True)]
    pallas_call x0 -> x1, Pallas kernels: none -> 128 us  [on_device(): pl.pallas_call(functools.partial(exchange, gr_size, sp_size), out_shape=(...]
    all_gather x2 -> x0, blocking collectives: 74 us -> none  [the longest x1 43.3 us: gathered(): return lax.all_gather(part, axis, axis=dim, tiled=True)]
    all_to_all x3 -> x0, waiting for transfers between devices: 23 us -> none  [the longest x1 23 us: on_device(): lax.all_to_all(values, 'sp', split_axis=0, concat_axis=2, tiled=True)]
    dot_general x5 -> x2, matrix products: 22.4 us -> 3.21 us  [the longest x1 1.74 us: on_device(): jnp.einsum('hd,hpd->hp', query, key_cache, preferred_element_type=jnp.flo...]
    all_to_all x3 -> x0, starting transfers between devices: 10.7 us -> none  [the longest x1 3.78 us: on_device(): lax.all_to_all(values, 'sp', split_axis=0, concat_axis=2, tiled=True)]
    all_to_all x6 -> x0, local copies, waits for them, and re-layouts: 3.75 us -> none  [the longest x4 1.28 us: on_device(): lax.all_to_all(cumulative, 'sp', split_axis=0, concat_axis=2, tiled=True)]
  transfers between devices with their start and end apart: 5 -> 0, of which waited for: 3 -> 0; matrix products, arithmetic and copies ran while one was open for 10% -> 0% of each run, Pallas kernels for 0% -> 0%
where the time goes in v1:
time: 143 us; the launch traced here: 141 us
  Pallas kernels  128 us (90%)
  other arithmetic  6.14 us (4%)
  local copies, waits for them, and re-layouts  3.44 us (2%)
  matrix products  3.21 us (2%)
    pallas_call x1, Pallas kernels, on_device(): pl.pallas_call(functools.partial(exchange, gr_size, sp_size), out_shape=(...  128 us

profile of v1, /device:TPU:0, one launch (start us, length us, event | category | flops | bytes accessed | tf_op | source)
XLA Modules:
  0.0 141.4 jit_solution(17813453944140226605)
XLA Ops:
  0.6 0.0 copy-start
  0.6 0.0 copy-start.2
  0.7 0.7 copy-done
  1.4 2.3 %pad_maximum_fusion.weights = bf16[2,256,1024]{2,1,0:T(8,128)(2,1)} fusion(bf16[1,256,1024]{2,1,0:T(8,128)(2,1)} %bitcast.29, bf16[1,256,1024]{2,1,0:T(8,128)(2,1)} %bitcast.30), kind=kLoop, calls=%fused_computation | loop fusion | flops 524288 | bytes 2097152 | tf_op jit(solution)/shard_map/stack | solution.py:339
  3.6 0.0 copy-done.2
  3.6 0.6 convert_bitcast_fusion.gate_rows
  4.2 0.0 copy-start.3
  4.2 127.9 %shard_map.93 = (bf16[16,512,128]{2,1,0:T(8,128)(2,1)}, f32[8,8,64]{2,1,0:T(8,128)}) custom-call(bf16[8,64,4096]{2,1,0:T(8,128)(2,1)} %tokens.1, bf16[2,256,1024]{2,1,0:T(8,128)(2,1)} %pad_maximum_fusion.weights, f32[8,256]{1,0:T(8,128)} %convert_bitcast_fusion.gate_rows), custom_call_target="tpu_custom_call" | custom-call | tf_op jit(solution)/shard_map/pallas_call | solution.py:343
  132.1 0.0 copy-start.1
  132.1 1.7 %fusion.2 = f32[8,1,512]{2,1,0:T(1,128)S(1)} fusion(bf16[16,512,128]{2,1,0:T(8,128)(2,1)} %get-tuple-element.6, bf16[8,128,1]{1,0,2:T(8,128)(2,1)S(1)} %dynamic-slice_bitcast_fusion), kind=kOutput, calls=%fused_computation.4 | convolution fusion | flops 1048576 | bytes 1067008 | tf_op jit(solution)/shard_map/hd,hpd->hp/dot_general | solution.py:375
  133.9 0.8 copy.14
  134.6 0.1 reshape.58
  134.7 0.0 copy-done.3
  134.7 0.1 fusion.4
  134.8 1.1 reduce-window.6
  136.0 0.2 slice_reduce_fusion
  136.2 0.7 add_bitcast_fusion
  136.8 0.2 slice_reduce_fusion.1
  137.0 0.2 fusion.13
  137.2 0.1 fusion.10
  137.3 1.5 %fusion = f32[8,1,128]{2,1,0:T(1,128)S(1)} fusion(bf16[16,512,128]{2,1,0:T(8,128)(2,1)} %get-tuple-element.6, bf16[8,512,1]{1,0,2:T(8,128)(2,1)S(1)} %fusion.10), kind=kOutput, calls=%fused_computation.1 | convolution fusion | flops 1048576 | bytes 1060864 | tf_op jit(solution)/shard_map/hp,hpd->hd/dot_general | solution.py:381
  138.8 0.2 fusion.9
  139.0 0.2 multiply_reduce_fusion
  139.2 0.7 fusion.12
  139.8 0.0 copy-done.1
  139.8 1.5 %slice_bitcast_fusion = (bf16[1,8,512,128]{3,2,1,0:T(8,128)(2,1)}, bf16[1,8,512,128]{3,2,1,0:T(8,128)(2,1)}) fusion(bf16[16,512,128]{2,1,0:T(8,128)(2,1)S(1)} %copy-done.1), kind=kLoop, calls=%fused_computation.3 | loop fusion | bytes 4194304 | tf_op jit(solution)/shard_map/broadcast_in_dim | solution.py:384
  (4 shorter events, 0.0 us)
Async XLA Ops:
  0.6 0.7 copy-start
  0.6 3.0 %copy-start.2 = (bf16[256,8]{0,1:T(8,128)(2,1)S(1)}, bf16[256,8]{0,1:T(8,128)(2,1)}, u32[]{:S(2)}) copy-start(bf16[256,8]{0,1:T(8,128)(2,1)} %param.9) | copy-start | bytes 12292
  4.2 130.5 %copy-start.3 = (f32[8]{0:T(128)S(1)}, f32[8]{0:T(128)}, u32[]{:S(2)}) copy-start(f32[8]{0:T(128)} %param.10) | copy-start | bytes 100
  132.1 7.7 %copy-start.1 = (bf16[16,512,128]{2,1,0:T(8,128)(2,1)S(1)}, bf16[16,512,128]{2,1,0:T(8,128)(2,1)}, u32[]{:S(2)}) copy-start(bf16[16,512,128]{2,1,0:T(8,128)(2,1)} %get-tuple-element.6) | copy-start | bytes 6291460

commit v2 on v1

v2 whole, which is shorter than its diff:
```python
import functools

import jax
import jax.numpy as jnp
from jax import lax
from jax.experimental import pallas as pl
from jax.experimental.pallas import tpu as pltpu
from jax.sharding import PartitionSpec as P

eps = 1e-06
MESH = pl.DeviceIdType.MESH


def exchange(
    gr_size, sp_size, tokens, key_weight, value_weight, gate_rows, kv_out, gate_out,
    tok, weights, full, gates, staged, gate_staged,
    tok_send, tok_recv, mate_send, mate_recv, w_send, w_recv, z_send, z_recv,
    gw_send, gw_recv, g_send, g_recv, o_send, o_recv, kept, local,
):
    g, s, t = lax.axis_index("gr"), lax.axis_index("sp"), lax.axis_index("tp")
    y, z = lax.rem(s, 2), s // 2
    levels = sp_size // 2
    sequences, positions, features = tokens.shape
    depth = weights.shape[1]
    parts, tile = full.shape[0], full.shape[2]
    width = parts * tile
    head_dim = kv_out.shape[2]
    heads = width // head_dim
    tile_heads = tile // head_dim
    members = gr_size * sp_size
    me = g * sp_size + s
    mate = t + 1 - 2 * lax.rem(t, 2)
    core = lax.rem(t, 2)
    quarter = sequences // 4

    gr_of = (g, 1 - g, g, 1 - g)
    y_of = (y, y, 1 - y, 1 - y)

    def where(r, level=None):
        return (gr_of[r], (z if level is None else level) * 2 + y_of[r], t)

    def remote(src, dst, send, recv, device):
        return pltpu.make_async_remote_copy(
            src_ref=src, dst_ref=dst, send_sem=send, recv_sem=recv,
            device_id=device, device_id_type=MESH,
        )

    taken = [
        pltpu.make_async_copy(ref, weights.at[k], local.at[k])
        for k, ref in enumerate((key_weight, value_weight))
    ]
    for copy in taken:
        copy.start()
    own_tokens = pltpu.make_async_copy(tokens, tok.at[0], local.at[2])
    own_tokens.start()
    own_gate = pltpu.make_async_copy(gate_rows, gates.at[me], local.at[3])
    own_gate.start()
    barrier = pltpu.get_barrier_semaphore()

    def greet(k, carry):
        @pl.when(k != me)
        def _():
            pl.semaphore_signal(
                barrier, inc=1, device_id=(k // sp_size, lax.rem(k, sp_size), t),
                device_id_type=MESH,
            )
        return carry

    lax.fori_loop(0, members, greet, 0)
    pl.semaphore_signal(barrier, inc=1, device_id=(g, s, mate), device_id_type=MESH)
    pl.semaphore_wait(barrier, members)

    def rows_at(r, level, c):
        return full.at[c, pl.ds(pl.multiple_of((gr_of[r] * sp_size + level * 2 + y_of[r]) * depth, depth), depth), :]

    def part_for(r, c):
        return weights.at[gr_of[r], :, pl.ds(pl.multiple_of(y_of[r] * width + c * tile, tile), tile)]

    def w_copy(r, c):
        return remote(part_for(r, c), rows_at(0, z, c), w_send.at[r, c], w_recv.at[r, c], where(r))

    def w_landing(r, c):
        return remote(part_for(r, c), rows_at(r, z, c), w_send.at[r, c], w_recv.at[r, c], where(r))

    def z_copy(direction, r, level, c, src=None):
        block = rows_at(r, level, c)
        to = z + 1 if direction == 0 else z - 1
        return remote(
            block if src is None else src, block, z_send.at[direction, level, r, c],
            z_recv.at[level, r, c], where(0, to),
        )

    def can_send(direction):
        return z < levels - 1 if direction == 0 else z > 0

    def pass_on(direction, r, level, c, src=None):
        @pl.when(can_send(direction))
        def _():
            z_copy(direction, r, level, c, src).start()

    def level_out(c):
        for direction in range(2):
            pass_on(direction, 0, z, c, part_for(0, c))
        for r in (1, 2, 3):
            w_landing(r, c).wait_recv()
            for direction in range(2):
                pass_on(direction, r, z, c)

    for copy in taken:
        copy.wait()
    for c in range(parts):
        for r in (3, 1, 2):
            w_copy(r, c).start()

    def gw_copy(k):
        return remote(
            gate_rows, gates.at[me], gw_send.at[k], gw_recv.at[me],
            (k // sp_size, lax.rem(k, sp_size), t),
        )

    def gw_landing(k):
        return remote(
            gate_rows, gates.at[k], gw_send.at[k], gw_recv.at[k],
            (k // sp_size, lax.rem(k, sp_size), t),
        )

    def others(fn):
        def turn(k, carry):
            @pl.when(k != me)
            def _():
                fn(k)
            return carry
        lax.fori_loop(0, members, turn, 0)

    others(lambda k: gw_copy(k).start())
    def piece(ref, half, c):
        return ref.at[pl.ds((half * 2 + c) * quarter, quarter)]

    def tok_copy(r, c):
        return remote(
            piece(tokens, core, c), piece(tok.at[r], core, c),
            tok_send.at[r, c], tok_recv.at[r, c], where(r),
        )

    def corner_copy(via, c):
        return remote(
            piece(tok.at[via], core, c), piece(tok.at[3], core, c),
            tok_send.at[3, c], tok_recv.at[3, c], where(3 - via),
        )

    def mate_copy(r, c, half):
        return remote(
            piece(tok.at[r], half, c), piece(tok.at[r], half, c),
            mate_send.at[r, c], mate_recv.at[r, c], (g, s, mate),
        )

    for c in range(2):
        tok_copy(1, c).start()
        tok_copy(2, 1 - c).start()

    def token_arrival(r, c):
        tok_copy(r, c).wait_recv()
        mate_copy(r, c, core).start()

    level_out(0)
    own_gate.wait()
    own_tokens.wait()

    others(lambda k: gw_landing(k).wait_recv())
    gate_full = jnp.concatenate([gates[k] for k in range(members)], axis=1).astype(jnp.bfloat16)

    def gate_copy(k):
        return remote(
            gate_staged.at[k], gate_out.at[s], g_send.at[k], g_recv.at[s], (g, k, t)
        )

    def gate_landing(k):
        return remote(
            gate_staged.at[k], gate_out.at[k], g_send.at[k], g_recv.at[k], (g, k, t)
        )

    def gate_turn(k, carry):
        gate_staged[k] = lax.dot_general(
            gate_full, tok[0, k], (((1,), (1,)), ((), ())),
            preferred_element_type=jnp.float32,
        )
        @pl.when(k != s)
        def _():
            gate_copy(k).start()
        @pl.when(k == s)
        def _():
            pltpu.make_async_copy(gate_staged.at[k], gate_out.at[k], local.at[4]).start()
        return carry

    lax.fori_loop(0, sequences, gate_turn, 0)

    def z_step(j, c):
        for r in range(4):
            @pl.when(z - j >= 0)
            def _():
                z_copy(0, r, z - j, c).wait_recv()
                pass_on(0, r, z - j, c)
            @pl.when(z + j < levels)
            def _():
                z_copy(1, r, z + j, c).wait_recv()
                pass_on(1, r, z + j, c)

    group = min(sequences, max(1, 512 // positions))
    groups = sequences // group

    def cache_at(their_g, their_y, their_z, b, c):
        return kv_out.at[
            pl.ds((their_g * 2 + their_y) * heads + c * tile_heads, tile_heads),
            pl.ds(pl.multiple_of((their_z * 2 + b) * positions, positions), positions),
            :,
        ]

    def out_copy(r, k, c):
        return remote(
            staged.at[r, c, :, k], cache_at(g, y, z, y_of[r], c),
            o_send.at[r, k, c], o_recv.at[me, y_of[r], c], (gr_of[r], k, t),
        )

    def out_landing(k, b, c):
        their_g, their_s = k // sp_size, lax.rem(k, sp_size)
        their_y, their_z = lax.rem(their_s, 2), their_s // 2
        return remote(
            staged.at[0, c, :, 0], cache_at(their_g, their_y, their_z, b, c),
            o_send.at[0, 0, c], o_recv.at[k, b, c], (their_g, their_s, t),
        )

    def keep_copy(r, c):
        return pltpu.make_async_copy(
            staged.at[r, c, :, s], cache_at(g, y, z, y_of[r], c), kept.at[r, c]
        )

    def products(r, c):
        def turn(m, carry):
            rows = tok[r, pl.ds(m * group, group)].reshape(group * positions, features)
            out = jnp.dot(rows, full[c], preferred_element_type=jnp.float32).astype(jnp.bfloat16)
            for h in range(tile_heads):
                staged[r, c, h, pl.ds(m * group, group)] = out[
                    :, h * head_dim : (h + 1) * head_dim
                ].reshape(group, positions, head_dim)
            return carry

        lax.fori_loop(0, groups, turn, 0)

        def send(i, carry):
            k = lax.rem(s + 1 + i, sp_size)
            if r in (1, 3):
                out_copy(r, k, c).start()
            else:
                @pl.when(k != s)
                def _():
                    out_copy(r, k, c).start()
                @pl.when(k == s)
                def _():
                    keep_copy(r, c).start()
            return carry

        lax.fori_loop(0, sequences, send, 0)

    def keep_rows(c):
        at = pl.multiple_of(me * depth, depth)
        columns = pl.ds(pl.multiple_of(y * width + c * tile, tile), tile)
        full[c, pl.ds(at, depth), :] = weights[g, :, columns]

    for c in range(parts):
        keep_rows(c)
    last = levels - 1
    for j in range(1, last):
        z_step(j, 0)
    for c in range(1, parts):
        level_out(c)
    token_arrival(1, 0)
    corner_copy(1, 0).start()
    token_arrival(2, 1)
    corner_copy(2, 1).start()
    z_step(last, 0)
    products(0, 0)
    for c in range(1, parts):
        z_step(1, c) if last > 1 else None
    token_arrival(1, 1)
    token_arrival(2, 0)
    for c in range(1, parts):
        for j in range(2, last):
            z_step(j, c)
    for r in (1, 2):
        for c in range(2):
            mate_copy(r, c, 1 - core).wait_recv()
        products(r, 0)
    for c in range(1, parts):
        z_step(last, c)
        for r in (0, 1, 2):
            products(r, c)
    for c in range(2):
        token_arrival(3, c)
    for c in range(2):
        mate_copy(3, c, 1 - core).wait_recv()
    for c in range(parts):
        products(3, c)

    def landed(k):
        for b in range(2):
            for c in range(parts):
                out_landing(k, b, c).wait_recv()

    others(landed)
    for c in range(parts):
        keep_copy(0, c).wait()
        keep_copy(2, c).wait()

    def gate_landed(k, carry):
        @pl.when(k != s)
        def _():
            gate_landing(k).wait_recv()
            gate_copy(k).wait_send()
        @pl.when(k == s)
        def _():
            pltpu.make_async_copy(gate_staged.at[k], gate_out.at[k], local.at[4]).wait()
        return carry

    lax.fori_loop(0, sequences, gate_landed, 0)
    others(lambda k: gw_copy(k).wait_send())
    for r in (1, 2, 3):
        for c in range(parts):
            w_copy(r, c).wait_send()
        for c in range(2):
            mate_copy(r, c, core).wait_send()
    for c in range(2):
        tok_copy(1, c).wait_send()
        tok_copy(2, c).wait_send()
    corner_copy(1, 0).wait_send()
    corner_copy(2, 1).wait_send()
    for r in range(4):
        def sent(k, carry):
            for c in range(parts):
                if r in (1, 3):
                    out_copy(r, k, c).wait_send()
                else:
                    @pl.when(k != s)
                    def _():
                        out_copy(r, k, c).wait_send()
            return carry
        lax.fori_loop(0, sequences, sent, 0)
    for r in range(4):
        for c in range(parts):
            for direction in range(2):
                @pl.when(can_send(direction))
                def _():
                    z_copy(direction, r, z, c, part_for(0, c) if r == 0 else None).wait_send()
            for j in range(1, levels):
                @pl.when((z - j >= 0) & can_send(0))
                def _():
                    z_copy(0, r, z - j, c).wait_send()
                @pl.when((z + j < levels) & can_send(1))
                def _():
                    z_copy(1, r, z + j, c).wait_send()


def on_device(gr_size, sp_size, tokens, key_weight, value_weight, gate_weight, forget_bias, new_query):
    sequences, positions, features = tokens.shape
    heads_here = forget_bias.shape[0]
    head_dim = new_query.shape[2]
    scaling = head_dim ** (-0.5)
    members = gr_size * sp_size
    depth = key_weight.shape[0]
    width = 2 * key_weight.shape[1] // 4
    parts = 2 if width >= 2 * head_dim else 1
    tile = width // parts
    gate_rows = gate_weight.T.astype(jnp.float32)
    levels = sp_size // 2
    dma = pltpu.SemaphoreType.DMA
    kv, logits = pl.pallas_call(
        functools.partial(exchange, gr_size, sp_size),
        out_shape=(
            jax.ShapeDtypeStruct((2 * heads_here, sp_size * positions, head_dim), jnp.bfloat16),
            jax.ShapeDtypeStruct((sp_size, heads_here, positions), jnp.float32),
        ),
        in_specs=[pl.BlockSpec(memory_space=pl.ANY)] * 4,
        out_specs=(pl.BlockSpec(memory_space=pl.ANY),) * 2,
        scratch_shapes=[
            pltpu.VMEM((4, sequences, positions, features), jnp.bfloat16),
            pltpu.VMEM((2, depth, key_weight.shape[1]), jnp.bfloat16),
            pltpu.VMEM((parts, features, tile), jnp.bfloat16),
            pltpu.VMEM((members, heads_here, depth), jnp.float32),
            pltpu.VMEM((4, parts, tile // head_dim, sequences, positions, head_dim), jnp.bfloat16),
            pltpu.VMEM((sequences, heads_here, positions), jnp.float32),
            dma((4, 2)), dma((4, 2)), dma((4, 2)), dma((4, 2)),
            dma((4, parts)), dma((4, parts)),
            dma((2, levels, 4, parts)), dma((levels, 4, parts)),
            dma((members,)), dma((members,)),
            dma((sp_size,)), dma((sp_size,)),
            dma((4, sp_size, parts)), dma((members, 2, parts)),
            dma((4, parts)), dma((5,)),
        ],
        compiler_params=pltpu.CompilerParams(
            collective_id=0, has_side_effects=True, vmem_limit_bytes=60 * 1024 * 1024
        ),
    )(tokens, key_weight, value_weight, gate_rows)
    key_cache, value_cache = kv[:heads_here], kv[heads_here:]
    logit = logits.transpose(1, 0, 2).reshape(heads_here, sp_size * positions)
    log_gate = jax.nn.log_sigmoid(logit + forget_bias[:, None])
    cumulative = jnp.cumsum(log_gate, axis=1)
    query = lax.dynamic_index_in_dim(new_query, lax.axis_index("sp"), 0, keepdims=False)
    scores = (
        jnp.einsum("hd,hpd->hp", query, key_cache, preferred_element_type=jnp.float32) * scaling
        + cumulative[:, -1:] - cumulative
    )
    highest = jnp.max(scores, axis=1, keepdims=True)
    probs = jnp.exp(scores - highest)
    total = jnp.sum(probs, axis=1)
    attended = jnp.einsum("hp,hpd->hd", probs, value_cache.astype(jnp.float32)) / total[:, None]
    normed = attended * lax.rsqrt(jnp.mean(attended * attended, axis=-1, keepdims=True) + eps)
    return (
        key_cache[None], value_cache[None], cumulative[None], normed.astype(jnp.bfloat16)[None]
    )


def solution(mesh):
    in_specs = (
        P("gr", "sp", None),
        P(("gr", "sp"), "tp"),
        P(("gr", "sp"), "tp"),
        P(("gr", "sp"), "tp"),
        P("tp"),
        P("gr", "tp", None),
    )
    out_specs = (
        P(("gr", "sp"), "tp", None, None),
        P(("gr", "sp"), "tp", None, None),
        P(("gr", "sp"), "tp", None),
        P(("gr", "sp"), "tp", None),
    )
    return jax.shard_map(
        functools.partial(on_device, mesh.shape["gr"], mesh.shape["sp"]),
        mesh=mesh, in_specs=in_specs, out_specs=out_specs, check_vma=False,
    )
```

time: 143 us -> 137 us (0.958)
  Pallas kernels: 128 us -> 123 us
  other arithmetic: 6.14 us -> 4.56 us
    pallas_call x1, Pallas kernels: 128 us -> 123 us  [on_device(): pl.pallas_call(functools.partial(exchange, gr_size, sp_size), out_shape=(...]
    another operation x4 -> x3, other arithmetic: 4.13 us -> 1.87 us  [the longest x1 2.27 us: on_device(): weights = jnp.stack([key_weight, value_weight])]
where the time goes in v2:
time: 137 us; the launch traced here: 135 us
  Pallas kernels  123 us (90%)
  other arithmetic  4.56 us (3%)
  local copies, waits for them, and re-layouts  3.45 us (3%)
  matrix products  3.21 us (2%)
    pallas_call x1, Pallas kernels, on_device(): pl.pallas_call(functools.partial(exchange, gr_size, sp_size), out_shape=(...  123 us

profile of v2, /device:TPU:0, one launch (start us, length us, event | category | flops | bytes accessed | tf_op | source)
XLA Modules:
  0.0 135.1 jit_solution(16494165654676719930)
XLA Ops:
  0.6 0.0 copy-start
  0.6 0.7 copy-done
  1.4 1.3 convert_bitcast_fusion.gate_rows
  2.6 0.0 copy-start.2
  2.6 123.2 %shard_map.93 = (bf16[16,512,128]{2,1,0:T(8,128)(2,1)}, f32[8,8,64]{2,1,0:T(8,128)}) custom-call(bf16[8,64,4096]{2,1,0:T(8,128)(2,1)} %tokens.1, bf16[256,1024]{1,0:T(8,128)(2,1)} %key_weight.1, bf16[256,1024]{1,0:T(8,128)(2,1)} %value_weight.1, f32[8,256]{1,0:T(8,128)} %convert_bitcast_fusion.gate_rows), custom_call_target="tpu_custom_call" | custom-call | tf_op jit(solution)/shard_map/pallas_call | solution.py:375
  125.8 0.0 copy-start.1
  125.8 1.7 %fusion.2 = f32[8,1,512]{2,1,0:T(1,128)S(1)} fusion(bf16[16,512,128]{2,1,0:T(8,128)(2,1)} %get-tuple-element.6, bf16[8,128,1]{1,0,2:T(8,128)(2,1)S(1)} %dynamic-slice_bitcast_fusion), kind=kOutput, calls=%fused_computation.3 | convolution fusion | flops 1048576 | bytes 1067008 | tf_op jit(solution)/shard_map/hd,hpd->hp/dot_general | solution.py:408
  127.6 0.8 copy.14
  128.3 0.1 reshape.58
  128.4 0.0 copy-done.2
  128.4 0.1 fusion.4
  128.5 1.1 reduce-window.6
  129.7 0.2 slice_reduce_fusion
  129.9 0.7 add_bitcast_fusion
  130.5 0.2 slice_reduce_fusion.1
  130.7 0.2 fusion.13
  130.9 0.1 fusion.10
  131.0 1.5 %fusion = f32[8,1,128]{2,1,0:T(1,128)S(1)} fusion(bf16[16,512,128]{2,1,0:T(8,128)(2,1)} %get-tuple-element.6, bf16[8,512,1]{1,0,2:T(8,128)(2,1)S(1)} %fusion.10), kind=kOutput, calls=%fused_computation | convolution fusion | flops 1048576 | bytes 1060864 | tf_op jit(solution)/shard_map/hp,hpd->hd/dot_general | solution.py:414
  132.5 0.2 fusion.9
  132.7 0.2 multiply_reduce_fusion
  132.9 0.7 fusion.12
  133.5 0.0 copy-done.1
  133.5 1.5 %slice_bitcast_fusion = (bf16[1,8,512,128]{3,2,1,0:T(8,128)(2,1)}, bf16[1,8,512,128]{3,2,1,0:T(8,128)(2,1)}) fusion(bf16[16,512,128]{2,1,0:T(8,128)(2,1)S(1)} %copy-done.1), kind=kLoop, calls=%fused_computation.2 | loop fusion | bytes 4194304 | tf_op jit(solution)/shard_map/broadcast_in_dim | solution.py:417
  (4 shorter events, 0.0 us)
Async XLA Ops:
  0.6 0.7 copy-start
  2.6 125.8 %copy-start.2 = (f32[8]{0:T(128)S(1)}, f32[8]{0:T(128)}, u32[]{:S(2)}) copy-start(f32[8]{0:T(128)} %param.10) | copy-start | bytes 100
  125.8 7.7 %copy-start.1 = (bf16[16,512,128]{2,1,0:T(8,128)(2,1)S(1)}, bf16[16,512,128]{2,1,0:T(8,128)(2,1)}, u32[]{:S(2)}) copy-start(bf16[16,512,128]{2,1,0:T(8,128)(2,1)} %get-tuple-element.6) | copy-start | bytes 6291460

commit v3 on v2

--- a/solution.py
+++ b/solution.py
@@ -292,10 +292,12 @@
         products(r, 0)
     for c in range(1, parts):
         z_step(last, c)
-        for r in (0, 1, 2):
+        for r in (0, 1):
             products(r, c)
     for c in range(2):
         token_arrival(3, c)
+    for c in range(1, parts):
+        products(2, c)
     for c in range(2):
         mate_copy(3, c, 1 - core).wait_recv()
     for c in range(parts):

time: 137 us -> 136 us (level)
  no operation moved by 1% of the time
where the time goes in v3:
time: 136 us; the launch traced here: 135 us
  Pallas kernels  123 us (90%)
  other arithmetic  4.56 us (3%)
  local copies, waits for them, and re-layouts  3.45 us (3%)
  matrix products  3.21 us (2%)
    pallas_call x1, Pallas kernels, on_device(): pl.pallas_call(functools.partial(exchange, gr_size, sp_size), out_shape=(...  123 us

profile of v3, /device:TPU:0, one launch (start us, length us, event | category | flops | bytes accessed | tf_op | source)
XLA Modules:
  0.0 135.3 jit_solution(8214482832241540823)
XLA Ops:
  0.6 0.0 copy-start
  0.6 0.7 copy-done
  1.4 1.3 convert_bitcast_fusion.gate_rows
  2.6 0.0 copy-start.2
  2.6 123.4 %shard_map.93 = (bf16[16,512,128]{2,1,0:T(8,128)(2,1)}, f32[8,8,64]{2,1,0:T(8,128)}) custom-call(bf16[8,64,4096]{2,1,0:T(8,128)(2,1)} %tokens.1, bf16[256,1024]{1,0:T(8,128)(2,1)} %key_weight.1, bf16[256,1024]{1,0:T(8,128)(2,1)} %value_weight.1, f32[8,256]{1,0:T(8,128)} %convert_bitcast_fusion.gate_rows), custom_call_target="tpu_custom_call" | custom-call | tf_op jit(solution)/shard_map/pallas_call | solution.py:377
  126.0 0.0 copy-start.1
  126.1 1.7 %fusion.2 = f32[8,1,512]{2,1,0:T(1,128)S(1)} fusion(bf16[16,512,128]{2,1,0:T(8,128)(2,1)} %get-tuple-element.6, bf16[8,128,1]{1,0,2:T(8,128)(2,1)S(1)} %dynamic-slice_bitcast_fusion), kind=kOutput, calls=%fused_computation.3 | convolution fusion | flops 1048576 | bytes 1067008 | tf_op jit(solution)/shard_map/hd,hpd->hp/dot_general | solution.py:410
  127.8 0.8 copy.14
  128.6 0.1 reshape.58
  128.7 0.0 copy-done.2
  128.7 0.1 fusion.4
  128.8 1.1 reduce-window.6
  129.9 0.2 slice_reduce_fusion
  130.1 0.7 add_bitcast_fusion
  130.8 0.2 slice_reduce_fusion.1
  131.0 0.2 fusion.13
  131.2 0.1 fusion.10
  131.2 1.5 %fusion = f32[8,1,128]{2,1,0:T(1,128)S(1)} fusion(bf16[16,512,128]{2,1,0:T(8,128)(2,1)} %get-tuple-element.6, bf16[8,512,1]{1,0,2:T(8,128)(2,1)S(1)} %fusion.10), kind=kOutput, calls=%fused_computation | convolution fusion | flops 1048576 | bytes 1060864 | tf_op jit(solution)/shard_map/hp,hpd->hd/dot_general | solution.py:416
  132.7 0.2 fusion.9
  132.9 0.2 multiply_reduce_fusion
  133.1 0.7 fusion.12
  133.8 0.0 copy-done.1
  133.8 1.5 %slice_bitcast_fusion = (bf16[1,8,512,128]{3,2,1,0:T(8,128)(2,1)}, bf16[1,8,512,128]{3,2,1,0:T(8,128)(2,1)}) fusion(bf16[16,512,128]{2,1,0:T(8,128)(2,1)S(1)} %copy-done.1), kind=kLoop, calls=%fused_computation.2 | loop fusion | bytes 4194304 | tf_op jit(solution)/shard_map/broadcast_in_dim | solution.py:419
  (4 shorter events, 0.0 us)
Async XLA Ops:
  0.6 0.7 copy-start
  2.6 126.0 %copy-start.2 = (f32[8]{0:T(128)S(1)}, f32[8]{0:T(128)}, u32[]{:S(2)}) copy-start(f32[8]{0:T(128)} %param.10) | copy-start | bytes 100
  126.0 7.7 %copy-start.1 = (bf16[16,512,128]{2,1,0:T(8,128)(2,1)S(1)}, bf16[16,512,128]{2,1,0:T(8,128)(2,1)}, u32[]{:S(2)}) copy-start(bf16[16,512,128]{2,1,0:T(8,128)(2,1)} %get-tuple-element.6) | copy-start | bytes 6291460
